TPU v7x, 32 devices: a whole 2x2x4 slice. The times are simulated.
32 devices in a mesh: sp: 8 (over z, y), tp: 4 (over x, core).
Axes of the slice: x: 2, y: 2, z: 4, core: 2. Of those that a mesh axis runs over, the one named last changes fastest.
Arguments:
- resid: bfloat16 [6144, 2048], P(('sp', 'tp')), may hold values from -6 to 6
- query_small: bfloat16 [6144, 768], P('sp', 'tp'), may hold values from -480 to 480
- query_large: bfloat16 [6144, 1280], P('sp', 'tp'), may hold values from -480 to 480
- kv_latent: bfloat16 [6144, 256], P('sp'), may hold values from -6 to 6
- rope_key: bfloat16 [6144, 32], P('sp'), may hold values from -6 to 6
- kv_gain: bfloat16 [256], replicated, may hold values from 0.099609375 to 1.8984375
- up_key_small: bfloat16 [256, 512], P(None, 'tp'), may hold values from -0.375 to 0.375
- up_value_small: bfloat16 [256, 512], P(None, 'tp'), may hold values from -0.375 to 0.375
- up_key_large: bfloat16 [256, 1024], P(None, 'tp'), may hold values from -0.375 to 0.375
- up_value_large: bfloat16 [256, 1024], P(None, 'tp'), may hold values from -0.375 to 0.375
- out_weight: bfloat16 [1536, 2048], replicated, may hold values from -0.359375 to 0.359375
- mix_gain: bfloat16 [2048], replicated, may hold values from 0.099609375 to 1.8984375
- gate_weight: bfloat16 [2048, 5632], P('sp', 'tp'), may hold values from -0.125 to 0.125
- up_weight: bfloat16 [2048, 5632], P('sp', 'tp'), may hold values from -0.125 to 0.125
- down_weight: bfloat16 [2048, 5632], P('sp', 'tp'), may hold values from -0.078125 to 0.078125
Outputs:
- layer_output: bfloat16 [6144, 2048], P(('sp', 'tp'))
All inputs are finite; a program needn't handle non-finite values.
Results may differ from a plain program's by a relative error of at most 0.014.
The roundings to bfloat16 on the way count: a program that leaves them out, or rounds other values in their place, can miss the bound.
Values may be sent and summed in bfloat16 or wider, within the bound.
No kernel may reach another device: no remote copies, remote signals or barrier semaphores. Data moves between devices by JAX's collectives and lax.ppermute only.
A program may use at most 128 MiB of HBM per device.

v0:
```python
import math
import jax
import jax.numpy as jnp
from jax import lax
from jax.sharding import PartitionSpec as P

HEADS_SMALL = 8
NOPE_SMALL = 64
NOPE_LARGE = 128
VALUE_SMALL = 64
VALUE_LARGE = 128
ROTARY = 32
THETA = 10000.0
EPSILON = 1e-06
FLOOR = -1e30


def angles(positions, width):
    inverse = THETA ** (-jnp.arange(0, width, 2).astype(jnp.float32) / width)
    phase = positions.astype(jnp.float32)[:, None] * inverse[None, :]
    return (jnp.cos(phase), jnp.sin(phase))


def rotate(values, angle_cos, angle_sin):
    half = values.shape[-1] // 2
    first = values[..., :half].astype(jnp.float32)
    second = values[..., half:].astype(jnp.float32)
    turned = jnp.concatenate(
        [first * angle_cos - second * angle_sin, second * angle_cos + first * angle_sin], axis=-1
    )
    return turned.astype(jnp.bfloat16)


def norm_rows(values, gain):
    wide = values.astype(jnp.float32)
    scaled = wide * lax.rsqrt(jnp.mean(wide * wide, axis=-1, keepdims=True) + EPSILON)
    return (scaled * gain.astype(jnp.float32)).astype(jnp.bfloat16)


def split_query(query, heads, nope, angle_cos, angle_sin):
    shaped = query.reshape(query.shape[0], heads, -1)
    return (
        shaped[..., :nope],
        rotate(shaped[..., nope:], angle_cos[:, None, :], angle_sin[:, None, :]),
    )


def absorb(state, query_parts, key_nope, shared_block, values, offset, first, scale):
    query_nope, query_turned = query_parts
    scores = jnp.einsum("qhd,khd->hqk", query_nope, key_nope, preferred_element_type=jnp.float32)
    scores = scores + jnp.einsum(
        "qhd,kd->hqk", query_turned, shared_block, preferred_element_type=jnp.float32
    )
    scores = scores * scale
    query_pos = offset + jnp.arange(query_nope.shape[0], dtype=jnp.int32)
    key_pos = first + jnp.arange(key_nope.shape[0], dtype=jnp.int32)
    allowed = key_pos[None, :] <= query_pos[:, None]
    scores = jnp.where(allowed[None], scores, FLOOR)
    maximum, total, summed = state
    new_max = jnp.maximum(maximum, jnp.max(scores, axis=-1))
    weights = jnp.where(allowed[None], jnp.exp(scores - new_max[..., None]), 0.0)
    factor = jnp.exp(maximum - new_max)
    total = total * factor + jnp.sum(weights, axis=-1)
    summed = summed * factor[..., None] + jnp.einsum(
        "hqk,khd->hqd", weights.astype(jnp.bfloat16), values, preferred_element_type=jnp.float32
    )
    return (new_max, total, summed)


def finish(group_state):
    maximum, total, summed = group_state
    out = summed / total[..., None]
    return jnp.transpose(out, (1, 0, 2)).reshape(out.shape[1], -1).astype(jnp.bfloat16)


def on_device(
    resid,
    query_small,
    query_large,
    kv_latent,
    rope_key,
    kv_gain,
    up_key_small,
    up_value_small,
    up_key_large,
    up_value_large,
    out_weight,
    mix_gain,
    gate_weight,
    up_weight,
    down_weight,
):
    rows = kv_latent.shape[0]
    offset = lax.axis_index("sp") * rows
    last = offset + rows - 1
    positions = offset + jnp.arange(rows, dtype=jnp.int32)
    angle_cos, angle_sin = angles(positions, ROTARY)
    latent_normed = norm_rows(kv_latent, kv_gain)
    rotated_key = rotate(rope_key, angle_cos, angle_sin)
    heads_small = up_key_small.shape[1] // NOPE_SMALL
    heads_large = up_key_large.shape[1] // NOPE_LARGE
    small_parts = split_query(query_small, heads_small, NOPE_SMALL, angle_cos, angle_sin)
    large_parts = split_query(query_large, heads_large, NOPE_LARGE, angle_cos, angle_sin)
    scale_small = 1.0 / math.sqrt(NOPE_SMALL + ROTARY)
    scale_large = 1.0 / math.sqrt(NOPE_LARGE + ROTARY)

    def start_state(heads, width):
        return (
            jnp.full((heads, rows), FLOOR, jnp.float32),
            jnp.zeros((heads, rows), jnp.float32),
            jnp.zeros((heads, rows, width), jnp.float32),
        )

    initial = (start_state(heads_small, VALUE_SMALL), start_state(heads_large, VALUE_LARGE))

    def consume(state, keys_small, values_small, keys_large, values_large, shared_block, first):
        length = shared_block.shape[0]
        small = absorb(
            state[0],
            small_parts,
            keys_small.reshape(length, heads_small, NOPE_SMALL),
            shared_block,
            values_small.reshape(length, heads_small, VALUE_SMALL),
            offset,
            first,
            scale_small,
        )
        large = absorb(
            state[1],
            large_parts,
            keys_large.reshape(length, heads_large, NOPE_LARGE),
            shared_block,
            values_large.reshape(length, heads_large, VALUE_LARGE),
            offset,
            first,
            scale_large,
        )
        return (small, large)

    def expand(latent_block):
        return tuple(
            (
                jnp.dot(latent_block, matrix, preferred_element_type=jnp.float32).astype(
                    jnp.bfloat16
                )
                for matrix in (up_key_small, up_value_small, up_key_large, up_value_large)
            )
        )

    def from_latent(blocks):
        return expand(blocks[0]) + (blocks[1],)

    pieces = (
        lax.all_gather(latent_normed, "sp", axis=0, tiled=True),
        lax.all_gather(rotated_key, "sp", axis=0, tiled=True),
    )
    count = pieces[0].shape[0] // rows

    def step(index, inner):
        first = index * rows
        blocks = tuple((lax.dynamic_slice_in_dim(piece, index * rows, rows, 0) for piece in pieces))
        return lax.cond(
            first <= last,
            lambda held: consume(held, *from_latent(blocks), first),
            lambda held: held,
            inner,
        )

    state = lax.fori_loop(0, count, step, initial)
    attn_small = finish(state[0])
    attn_large = finish(state[1])
    border = HEADS_SMALL * VALUE_SMALL
    all_small, all_large = (
        lax.all_to_all(attn_small, "tp", split_axis=0, concat_axis=1, tiled=True),
        lax.all_to_all(attn_large, "tp", split_axis=0, concat_axis=1, tiled=True),
    )
    mixed = jnp.dot(all_small, out_weight[:border], preferred_element_type=jnp.float32)
    mixed = mixed + jnp.dot(all_large, out_weight[border:], preferred_element_type=jnp.float32)
    middle = (resid.astype(jnp.float32) + mixed).astype(jnp.bfloat16)
    mixer_in = norm_rows(middle, mix_gain)
    gate_whole, up_whole, down_whole = (
        lax.all_gather(gate_weight, "sp", axis=0, tiled=True),
        lax.all_gather(up_weight, "sp", axis=0, tiled=True),
        lax.all_gather(down_weight, "sp", axis=0, tiled=True),
    )
    piece = lax.all_gather(mixer_in, "tp", axis=0, tiled=True)
    gate = jnp.dot(piece, gate_whole, preferred_element_type=jnp.float32)
    upward = jnp.dot(piece, up_whole, preferred_element_type=jnp.float32)
    hidden = (jax.nn.silu(gate) * upward).astype(jnp.bfloat16)
    branch = lax.psum_scatter(
        lax.dot_general(
            hidden, down_whole, (((1,), (1,)), ((), ())), preferred_element_type=jnp.float32
        ).astype(jnp.bfloat16),
        "tp",
        scatter_dimension=0,
        tiled=True,
    ).astype(jnp.float32)
    return (middle.astype(jnp.float32) + branch).astype(jnp.bfloat16)


def solution(mesh):
    placed = (
        P(("sp", "tp"), None),
        P("sp", "tp"),
        P("sp", "tp"),
        P("sp", None),
        P("sp", None),
        P(),
        P(None, "tp"),
        P(None, "tp"),
        P(None, "tp"),
        P(None, "tp"),
        P(),
        P(),
        P("sp", "tp"),
        P("sp", "tp"),
        P("sp", "tp"),
    )
    return jax.shard_map(
        on_device, mesh=mesh, in_specs=placed, out_specs=P(("sp", "tp"), None), check_vma=False
    )
```

profile of v0, /device:TPU:0, one launch (start us, length us, event | category | flops | bytes accessed | tf_op | source)
XLA Modules:
  0.0 495.1 jit_solution(7308712939840525357)
XLA Ops:
  6.5 0.0 all-gather.6.cloned.1.call-start
  6.6 1.3 fusion.44
  7.9 0.7 convert_element_type.137
  8.5 1.9 fusion.46
  10.4 0.0 all-gather.6.cloned.1.call-update
  10.5 0.0 all-gather.10.cloned.1.call-start
  10.5 0.7 all-gather.10.cloned.1.call-update
  11.2 1.0 slice.49
  12.3 0.2 copy.33
  12.5 0.9 slice.46
  13.5 0.0 copy-done.4
  13.5 0.3 multiply_cosine_fusion
  13.8 0.9 fusion.56
  14.7 34.0 %all_gather.19 = bf16[6144,32]{0,1:T(8,128)(2,1)S(1)} all-gather(bf16[768,32]{0,1:T(8,128)(2,1)S(1)} %pad_maximum_fusion.2), channel_id=1, replica_groups=mesh['sp'=8,'tp'=4] {'sp'}, dimensions={0}, use_global_device_ids=true | all-gather | bytes 442368 | tf_op jit(solution)/shard_map/all_gather | solution.py:155
  48.8 26.8 %all-gather.6.cloned.1.call-done = bf16[6144,256]{1,0:T(8,128)(2,1)} async-done(((bf16[768,256]{1,0:T(8,128)(2,1)}), bf16[6144,256]{1,0:T(8,128)(2,1)}) %all-gather.6.cloned.1.call-update) | async-done | bytes 3145744 | tf_op jit(solution)/shard_map/all_gather | solution.py:154
  75.6 0.1 broadcast_in_dim.67
  75.7 0.0 copy-done.2
  75.7 0.0 copy-done.3
  75.8 0.0 copy-done
  75.8 0.0 copy-done.1
  75.8 0.0 copy-start.5
  75.8 15.2 %while.23 = (s32[]{:T(128)}, f32[2,768]{1,0:T(2,128)S(1)}, f32[2,768]{1,0:T(2,128)S(1)}, f32[2,768,64]{1,2,0:T(8,128)S(1)}, f32[2,768]{1,0:T(2,128)S(1)}, /*inde...) while((s32[]{:T(128)}, f32[2,768]{1,0:T(2,128)S(1)}, ...), condition=%wide.region_8.9_spmd, body=%wide.region_1.8_spmd.sunk | while | flops 1384324608 | bytes 58503696 | solution.py:169
  75.8 14.9 %conditional.2 = ((f32[2,768]{1,0:T(2,128)S(1)}, f32[2,768]{1,0:T(2,128)S(1)}, f32[2,768,64]{1,2,0:T(8,128)S(1)}, f32[2,768]{1,0:T(2,128)S(1)}, f32[2,768]{1,0:T(2,128)S(1)}, /*index=5*/f32[2,768,128]{2,1,0:T(8,128)S(1)})) conditional(s32[]{:T(128)} %convert_element_type.251, (f32[2,768]{1,0:T(2,128)S(1)}, f32[2,768]{1,0:T(2,128)S(1)}, ...), branch_computations={%region_2.0_spmd, %region_3.7_spmd} | conditional | flops 1384324608 | bytes 58503288 | solution.py:162
  75.8 1.3 convolution_convert_fusion.1
  77.2 0.8 fusion.67
  78.0 0.4 broadcast_compare_fusion
  78.4 1.3 fusion.65
  79.7 1.3 convolution_convert_fusion.3
  81.0 0.8 fusion.66
  81.9 1.3 fusion.64
  83.2 1.8 fusion.7
  85.0 1.3 convolution_convert_fusion
  86.3 1.8 fusion.16
  88.1 1.3 convolution_convert_fusion.2
  89.4 1.3 fusion.19
  91.0 0.3 fusion.47
  91.3 0.4 copy.36
  91.7 1.0 convert_element_type.152
  92.7 3.5 all-to-all-start.1
  96.2 0.0 copy-done.5
  96.3 0.2 convert_element_type.149
  96.5 0.9 copy.34
  97.4 6.2 %all-to-all-done.1 = bf16[4,192,256]{2,1,0:T(8,128)(2,1)S(1)} async-done(((bf16[4,192,256]{2,1,0:T(8,128)(2,1)}), bf16[4,192,256]{2,1,0:T(8,128)(2,1)S(1)}, u32[]{:S(2)}, u32[]{:S(2)}) %all-to-all-start.1) | async-done | bytes 393248 | tf_op jit(solution)/shard_map/all_to_all | solution.py:175
  103.6 3.4 all-to-all-start
  107.0 0.2 all-gather.8.cloned.1.call-start
  107.2 3.2 fusion.38
  110.4 1.8 all-to-all-done
  112.2 2.5 multiply_reduce_fusion
  114.8 1.1 multiply_convert_fusion.1
  115.8 0.0 all-gather.8.cloned.1.call-update
  115.9 0.0 all-gather.12.cloned.1.call-start
  115.9 0.5 all-gather.12.cloned.1.call-update
  116.4 0.0 all-gather.14.cloned.1.call-start
  116.5 0.5 all-gather.14.cloned.1.call-update
  117.0 0.0 reduce-scatter.2.cloned.1.call-start
  117.1 52.0 %all-gather.10.cloned.1.call-done = bf16[2048,1408]{1,0:T(8,128)(2,1)} async-done(((bf16[256,1408]{1,0:T(8,128)(2,1)}), bf16[2048,1408]{1,0:T(8,128)(2,1)}) %all-gather.10.cloned.1.call-update) | async-done | bytes 5767184 | tf_op jit(solution)/shard_map/all_gather | solution.py:182
  169.0 77.1 %all-gather.8.cloned.1.call-done = bf16[768,2048]{1,0:T(8,128)(2,1)} async-done(((bf16[192,2048]{1,0:T(8,128)(2,1)}), bf16[768,2048]{1,0:T(8,128)(2,1)}) %all-gather.8.cloned.1.call-update) | async-done | bytes 3145744 | tf_op jit(solution)/shard_map/all_gather | solution.py:186
  246.1 9.7 %fusion.68 = f32[768,1408]{1,0:T(8,128)} fusion(bf16[768,2048]{1,0:T(8,128)(2,1)} %all-gather.8.cloned.1.call-done, bf16[2048,1408]{1,0:T(8,128)(2,1)} %all-gather.10.cloned.1.call-done), kind=kOutput, calls=%fused_computation.108 | convolution fusion | flops 4429185024 | bytes 13238272 | tf_op jit(solution)/shard_map/dot_general | solution.py:187
  255.8 84.7 %all-gather.12.cloned.1.call-done = bf16[2048,1408]{1,0:T(8,128)(2,1)} async-done(((bf16[256,1408]{1,0:T(8,128)(2,1)}), bf16[2048,1408]{1,0:T(8,128)(2,1)}) %all-gather.12.cloned.1.call-update) | async-done | bytes 5767184 | tf_op jit(solution)/shard_map/all_gather | solution.py:183
  340.5 92.6 %all-gather.14.cloned.1.call-done = bf16[2048,1408]{1,0:T(8,128)(2,1)} async-done(((bf16[256,1408]{1,0:T(8,128)(2,1)}), bf16[2048,1408]{1,0:T(8,128)(2,1)}) %all-gather.14.cloned.1.call-update) | async-done | bytes 5767184 | tf_op jit(solution)/shard_map/all_gather | solution.py:184
  433.1 16.7 %convolution_convert_fusion.4 = bf16[768,2048]{1,0:T(8,128)(2,1)} fusion(bf16[2048,1408]{1,0:T(8,128)(2,1)} %all-gather.14.cloned.1.call-done, f32[768,1408]{1,0:T(8,128)} %fusion.68, bf16[768,2048]{1,0:T(8,128)(2,1)} %all-gather.8.cloned.1.call-done, bf16[2048,1408]{1,0:T(8,128)(2,1)} %all-gather.12.cloned.1.call-done), kind=kOutput, calls=%fused_computation.50 | convolution fusion | flops 8866430976 | bytes 22151168 | tf_op jit(solution)/shard_map/dot_general | solution.py:191
  449.8 0.0 reduce-scatter.2.cloned.1.call-update
  449.8 36.2 %reduce-scatter.2.cloned.1.call-done = bf16[192,2048]{1,0:T(8,128)(2,1)} async-done(((bf16[768,2048]{1,0:T(8,128)(2,1)}), bf16[192,2048]{1,0:T(8,128)(2,1)}) %reduce-scatter.2.cloned.1.call-update) | async-done | bytes 786448 | tf_op jit(solution)/shard_map/reduce_scatter | solution.py:190
  486.0 2.2 add_convert_fusion
  (33 shorter events, 0.3 us)
Async XLA Ops:
  6.5 6.9 %copy-start.4 = (bf16[768,32]{0,1:T(8,128)(2,1)S(1)}, bf16[768,32]{0,1:T(8,128)(2,1)}, u32[]{:S(2)}) copy-start(bf16[768,32]{0,1:T(8,128)(2,1)} %param.23) | copy-start | bytes 147460
  6.5 69.2 %copy-start.2 = (bf16[256,128]{1,0:T(8,128)(2,1)S(1)}, bf16[256,128]{1,0:T(8,128)(2,1)}, u32[]{:S(2)}) copy-start(bf16[256,128]{1,0:T(8,128)(2,1)} %param.25) | copy-start | bytes 196612
  6.5 69.2 %copy-start.3 = (bf16[256,128]{1,0:T(8,128)(2,1)S(1)}, bf16[256,128]{1,0:T(8,128)(2,1)}, u32[]{:S(2)}) copy-start(bf16[256,128]{1,0:T(8,128)(2,1)} %param.26) | copy-start | bytes 196612
  6.5 69.2 %copy-start = (bf16[256,256]{1,0:T(8,128)(2,1)S(1)}, bf16[256,256]{1,0:T(8,128)(2,1)}, u32[]{:S(2)}) copy-start(bf16[256,256]{1,0:T(8,128)(2,1)} %param.27) | copy-start | bytes 393220
  6.5 69.2 %copy-start.1 = (bf16[256,256]{1,0:T(8,128)(2,1)S(1)}, bf16[256,256]{1,0:T(8,128)(2,1)}, u32[]{:S(2)}) copy-start(bf16[256,256]{1,0:T(8,128)(2,1)} %param.28) | copy-start | bytes 393220
  6.5 69.0 %all-gather.6.cloned.1.call-start = ((), (), s32[]{:S(2)}) async-start(), calls=%async_computation.3 | async-start | bytes 3538944 | tf_op jit(solution)/shard_map/all_gather | solution.py:154
  10.5 158.6 %all-gather.10.cloned.1.call-start = ((), (), s32[]{:S(2)}) async-start(), calls=%async_computation.5 | async-start | bytes 6488064 | tf_op jit(solution)/shard_map/all_gather | solution.py:182
  75.8 20.4 %copy-start.5 = (bf16[2048]{0:T(1024)(128)(2,1)S(1)}, bf16[2048]{0:T(1024)(128)(2,1)}, u32[]{:S(2)}) copy-start(bf16[2048]{0:T(1024)(128)(2,1)} %param.30) | copy-start | bytes 12292
  92.7 10.8 %all-to-all-start.1 = ((bf16[4,192,256]{2,1,0:T(8,128)(2,1)}), bf16[4,192,256]{2,1,0:T(8,128)(2,1)S(1)}, u32[]{:S(2)}, u32[]{:S(2)}) async-start(bf16[4,192,256]{2,1,0:T(8,128)(2,1)} %convert_element_type.152), calls=%async_computation.1 | async-start | bytes 786432 | tf_op jit(solution)/shard_map/all_to_all | solution.py:175
  103.6 8.6 %all-to-all-start = ((bf16[4,192,128]{2,1,0:T(8,128)(2,1)}), bf16[4,192,128]{2,1,0:T(8,128)(2,1)S(1)}, u32[]{:S(2)}, u32[]{:S(2)}) async-start(bf16[4,192,128]{2,1,0:T(8,128)(2,1)} %copy.34), calls=%async_computation | async-start | bytes 393216 | tf_op jit(solution)/shard_map/all_to_all | solution.py:174
  107.0 139.2 %all-gather.8.cloned.1.call-start = ((), (), s32[]{:S(2)}) async-start(), calls=%async_computation.4 | async-start | bytes 3932160 | tf_op jit(solution)/shard_map/all_gather | solution.py:186
  115.9 224.7 %all-gather.12.cloned.1.call-start = ((), (), s32[]{:S(2)}) async-start(), calls=%async_computation.6 | async-start | bytes 6488064 | tf_op jit(solution)/shard_map/all_gather | solution.py:183
  116.4 316.6 %all-gather.14.cloned.1.call-start = ((), (), s32[]{:S(2)}) async-start(), calls=%async_computation.7 | async-start | bytes 6488064 | tf_op jit(solution)/shard_map/all_gather | solution.py:184
  117.0 369.0 %reduce-scatter.2.cloned.1.call-start = ((), (), s32[]{:S(2)}) async-start(), calls=%async_computation.8 | async-start | bytes 3932160 | tf_op jit(solution)/shard_map/reduce_scatter | solution.py:190
Sparse Core Ops, SparseCore 0:
  10.6 64.9 all-gather.5
  77.8 91.2 all-gather.9
  170.6 75.4 all-gather.7
  248.2 92.3 all-gather.11
  342.6 90.4 all-gather.13
  449.9 36.0 reduce-scatter.1
where the time goes:
time: 497 us; the launch traced here: 495 us
  waiting for transfers between devices  379 us (76%)
  matrix products  44.7 us (9%)
  blocking collectives  34 us (7%)
  between operations  13.7 us (3%)
  other arithmetic  10.9 us (2%)
  starting transfers between devices  7.25 us (1%)
    all_gather x1, waiting for transfers between devices, on_device(): lax.all_gather(down_weight, 'sp', axis=0, tiled=True)  92.6 us
    all_gather x1, waiting for transfers between devices, on_device(): lax.all_gather(up_weight, 'sp', axis=0, tiled=True)  84.7 us
    all_gather x1, waiting for transfers between devices, on_device(): piece = lax.all_gather(mixer_in, 'tp', axis=0, tiled=True)  77.1 us
    all_gather x1, waiting for transfers between devices, on_device(): lax.all_gather(gate_weight, 'sp', axis=0, tiled=True)  52 us
    reduce_scatter x1, waiting for transfers between devices, on_device(): lax.psum_scatter(lax.dot_general(hidden, down_whole, (((1,), (1,)), ((),...  36.2 us
    all_gather x1, blocking collectives, on_device(): lax.all_gather(rotated_key, 'sp', axis=0, tiled=True)  34 us
    all_gather x1, waiting for transfers between devices, on_device(): lax.all_gather(latent_normed, 'sp', axis=0, tiled=True)  26.8 us
    dot_general x1, matrix products, on_device(): lax.dot_general(hidden, down_whole, (((1,), (1,)), ((), ())), preferred_e...  16.7 us
  transfers between devices with their start and end apart: 8, of which 8 were waited for; matrix products, arithmetic and copies ran while one was open for 8% of the time, Pallas kernels for 0%

commit v1 on v0

--- a/solution.py
+++ b/solution.py
@@ -183,7 +183,12 @@
         lax.all_gather(up_weight, "sp", axis=0, tiled=True),
         lax.all_gather(down_weight, "sp", axis=0, tiled=True),
     )
-    piece = lax.all_gather(mixer_in, "tp", axis=0, tiled=True)
+    ring = [mixer_in]
+    for hop in range(3):
+        ring.append(lax.ppermute(ring[-1], "tp", [(dev, (dev + 1) % 4) for dev in range(4)]))
+    piece = jnp.roll(
+        jnp.concatenate(ring[::-1], axis=0), (lax.axis_index("tp") + 1) * ring[0].shape[0], axis=0
+    )
     gate = jnp.dot(piece, gate_whole, preferred_element_type=jnp.float32)
     upward = jnp.dot(piece, up_whole, preferred_element_type=jnp.float32)
     hidden = (jax.nn.silu(gate) * upward).astype(jnp.bfloat16)

time: 497 us -> 418 us (0.84)
  waiting for transfers between devices: 379 us -> 292 us
  local copies, waits for them, and re-layouts: 4.89 us -> 12 us
    all_gather x1 -> x0, waiting for transfers between devices: 77.1 us -> none  [on_device(): piece = lax.all_gather(mixer_in, 'tp', axis=0, tiled=True)]
    all_gather x1, waiting for transfers between devices: 52 us -> 9.36 us  [on_device(): lax.all_gather(gate_weight, 'sp', axis=0, tiled=True)]
    ppermute x0 -> x3, waiting for transfers between devices: none -> 34.3 us  [on_device(): lax.ppermute(ring[-1], 'tp', [(dev, (dev + 1) % 4) for dev in range(4)])]
    all_gather x1, waiting for transfers between devices: 92.6 us -> 83 us  [on_device(): lax.all_gather(down_weight, 'sp', axis=0, tiled=True)]
    unnamed x12 -> x20, local copies, waits for them, and re-layouts: 0.02 us -> 8.11 us
    all_gather x1, waiting for transfers between devices: 84.7 us -> 92.6 us  [on_device(): lax.all_gather(up_weight, 'sp', axis=0, tiled=True)]
  transfers between devices with their start and end apart: 8 -> 10, of which waited for: 8 -> 10; matrix products, arithmetic and copies ran while one was open for 8% -> 11% of each run, Pallas kernels for 0% -> 0%
where the time goes in v1:
time: 418 us; the launch traced here: 416 us
  waiting for transfers between devices  292 us (70%)
  matrix products  44.7 us (11%)
  blocking collectives  34.1 us (8%)
  between operations  13.4 us (3%)
  other arithmetic  12.2 us (3%)
  local copies, waits for them, and re-layouts  12 us (3%)
  starting transfers between devices  7.27 us (2%)
    all_gather x1, waiting for transfers between devices, on_device(): lax.all_gather(up_weight, 'sp', axis=0, tiled=True)  92.6 us
    all_gather x1, waiting for transfers between devices, on_device(): lax.all_gather(down_weight, 'sp', axis=0, tiled=True)  83 us
    reduce_scatter x1, waiting for transfers between devices, on_device(): lax.psum_scatter(lax.dot_general(hidden, down_whole, (((1,), (1,)), ((),...  36.2 us
    ppermute x3, waiting for transfers between devices, on_device(): lax.ppermute(ring[-1], 'tp', [(dev, (dev + 1) % 4) for dev in range(4)])  34.3 us
    all_gather x1, blocking collectives, on_device(): lax.all_gather(rotated_key, 'sp', axis=0, tiled=True)  34.1 us
    all_gather x1, waiting for transfers between devices, on_device(): lax.all_gather(latent_normed, 'sp', axis=0, tiled=True)  26.4 us
    dot_general x1, matrix products, on_device(): lax.dot_general(hidden, down_whole, (((1,), (1,)), ((), ())), preferred_e...  16.8 us
    dot_general x1, matrix products, on_device(): gate = jnp.dot(piece, gate_whole, preferred_element_type=jnp.float32)  9.69 us
  transfers between devices with their start and end apart: 10, of which 10 were waited for; matrix products, arithmetic and copies ran while one was open for 11% of the time, Pallas kernels for 0%

profile of v1, /device:TPU:0, one launch (start us, length us, event | category | flops | bytes accessed | tf_op | source)
XLA Modules:
  0.0 416.3 jit_solution(11130720606319636396)
XLA Ops:
  6.6 0.0 all-gather.5.cloned.1.call-start
  6.6 1.2 fusion.52
  7.9 0.7 convert_element_type.137
  8.5 1.9 fusion.54
  10.4 0.0 all-gather.5.cloned.1.call-update
  10.4 0.0 all-gather.7.cloned.1.call-start
  10.5 0.7 all-gather.7.cloned.1.call-update
  11.2 0.0 all-gather.11.cloned.1.call-start
  11.2 0.7 all-gather.11.cloned.1.call-update
  11.9 0.0 all-gather.9.cloned.1.call-start
  12.0 0.5 all-gather.9.cloned.1.call-update
  12.5 1.0 slice.49
  13.5 0.2 copy.33
  13.8 0.3 multiply_cosine_fusion
  14.1 0.9 fusion.64
  15.0 34.1 %all_gather.16 = bf16[6144,32]{0,1:T(8,128)(2,1)S(1)} all-gather(bf16[768,32]{0,1:T(8,128)(2,1)S(1)} %pad_maximum_fusion.2), channel_id=1, replica_groups=mesh['sp'=8,'tp'=4] {'sp'}, dimensions={0}, use_global_device_ids=true | all-gather | bytes 442368 | tf_op jit(solution)/shard_map/all_gather | solution.py:155
  49.2 26.4 %all-gather.5.cloned.1.call-done = bf16[6144,256]{1,0:T(8,128)(2,1)} async-done(((bf16[768,256]{1,0:T(8,128)(2,1)}), bf16[6144,256]{1,0:T(8,128)(2,1)}) %all-gather.5.cloned.1.call-update) | async-done | bytes 3145744 | tf_op jit(solution)/shard_map/all_gather | solution.py:154
  75.6 0.1 broadcast_in_dim.67
  75.8 15.3 %while.23 = (s32[]{:T(128)}, f32[2,768]{1,0:T(2,128)S(1)}, f32[2,768]{1,0:T(2,128)S(1)}, f32[2,768,64]{1,2,0:T(8,128)S(1)}, f32[2,768]{1,0:T(2,128)S(1)}, /*inde...) while((s32[]{:T(128)}, f32[2,768]{1,0:T(2,128)S(1)}, ...), condition=%wide.region_8.9_spmd, body=%wide.region_1.8_spmd.sunk | while | flops 1384324608 | bytes 58503696 | solution.py:169
  75.8 14.9 %conditional.2 = ((f32[2,768]{1,0:T(2,128)S(1)}, f32[2,768]{1,0:T(2,128)S(1)}, f32[2,768,64]{1,2,0:T(8,128)S(1)}, f32[2,768]{1,0:T(2,128)S(1)}, f32[2,768]{1,0:T(2,128)S(1)}, /*index=5*/f32[2,768,128]{2,1,0:T(8,128)S(1)})) conditional(s32[]{:T(128)} %convert_element_type.255, (f32[2,768]{1,0:T(2,128)S(1)}, f32[2,768]{1,0:T(2,128)S(1)}, ...), branch_computations={%region_2.0_spmd, %region_3.7_spmd} | conditional | flops 1384324608 | bytes 58503288 | solution.py:162
  75.8 1.3 convolution_convert_fusion.1
  77.1 0.8 fusion.78
  78.0 0.4 broadcast_compare_fusion
  78.4 1.3 fusion.76
  79.7 1.3 convolution_convert_fusion.3
  81.0 0.8 fusion.77
  81.8 1.2 fusion.75
  83.1 1.8 fusion.7
  84.9 1.3 convolution_convert_fusion
  86.3 1.8 fusion.16
  88.1 1.3 convolution_convert_fusion.2
  89.4 1.3 fusion.19
  91.1 0.3 fusion.55
  91.4 0.4 copy.36
  91.8 1.0 convert_element_type.152
  92.8 3.5 all-to-all-start.1
  96.3 0.2 convert_element_type.149
  96.5 0.9 copy.34
  97.4 6.2 %all-to-all-done.1 = bf16[4,192,256]{2,1,0:T(8,128)(2,1)S(1)} async-done(((bf16[4,192,256]{2,1,0:T(8,128)(2,1)}), bf16[4,192,256]{2,1,0:T(8,128)(2,1)S(1)}, u32[]{:S(2)}, u32[]{:S(2)}) %all-to-all-start.1) | async-done | bytes 393248 | tf_op jit(solution)/shard_map/all_to_all | solution.py:175
  103.6 3.5 all-to-all-start
  107.2 0.0 reduce-scatter.2.cloned.1.call-start
  107.3 3.2 fusion.38
  110.4 2.0 all-to-all-done
  112.4 2.6 multiply_reduce_fusion
  115.0 0.2 multiply_convert_fusion.1
  115.3 0.1 collective-permute-start
  115.3 11.4 %collective-permute-done = bf16[192,2048]{1,0:T(8,128)(2,1)S(1)} collective-permute-done((bf16[192,2048]{1,0:T(8,128)(2,1)S(1)}, bf16[192,2048]{1,0:T(8,128)(2,1)S(1)}, u32[]{:S(2)}, u32[]{:S(2)}) %collective-permute-start) | collective-permute-done | bytes 786464 | tf_op jit(solution)/shard_map/ppermute | solution.py:188
  126.7 11.4 %collective-permute-done.1 = bf16[192,2048]{1,0:T(8,128)(2,1)S(1)} collective-permute-done((bf16[192,2048]{1,0:T(8,128)(2,1)S(1)}, bf16[192,2048]{1,0:T(8,128)(2,1)S(1)}, u32[]{:S(2)}, u32[]{:S(2)}) %collective-permute-start.1) | collective-permute-done | bytes 786464 | tf_op jit(solution)/shard_map/ppermute | solution.py:188
  138.1 11.5 %collective-permute-done.2 = bf16[192,2048]{1,0:T(8,128)(2,1)} collective-permute-done((bf16[192,2048]{1,0:T(8,128)(2,1)S(1)}, bf16[192,2048]{1,0:T(8,128)(2,1)}, u32[]{:S(2)}, u32[]{:S(2)}) %collective-permute-start.2) | collective-permute-done | bytes 786464 | tf_op jit(solution)/shard_map/ppermute | solution.py:188
  149.7 2.1 constant_dynamic-update-slice_fusion.7
  151.7 1.0 constant_dynamic-update-slice_fusion.6
  152.7 0.9 constant_dynamic-update-slice_fusion.5
  153.7 1.1 constant_dynamic-update-slice_fusion.4
  154.8 2.1 constant_dynamic-update-slice_fusion.3
  156.9 1.0 constant_dynamic-update-slice_fusion.2
  157.9 1.0 constant_dynamic-update-slice_fusion.1
  158.8 1.1 constant_dynamic-update-slice_fusion
  159.9 9.4 %all-gather.7.cloned.1.call-done = bf16[2048,1408]{1,0:T(8,128)(2,1)} async-done(((bf16[256,1408]{1,0:T(8,128)(2,1)}), bf16[2048,1408]{1,0:T(8,128)(2,1)}) %all-gather.7.cloned.1.call-update) | async-done | bytes 5767184 | tf_op jit(solution)/shard_map/all_gather | solution.py:182
  169.3 9.7 %fusion.42 = f32[768,1408]{1,0:T(8,128)} fusion(bf16[2048,1408]{1,0:T(8,128)(2,1)} %all-gather.7.cloned.1.call-done, bf16[1536,2048]{1,0:T(8,128)(2,1)} %constant_dynamic-update-slice_fusion, s32[]{:T(128)S(6)} %select_n.49), kind=kOutput, calls=%fused_computation.53 | convolution fusion | flops 4429185024 | bytes 13238276 | tf_op jit(solution)/shard_map/dot_general | solution.py:192
  179.0 83.0 %all-gather.11.cloned.1.call-done = bf16[2048,1408]{1,0:T(8,128)(2,1)} async-done(((bf16[256,1408]{1,0:T(8,128)(2,1)}), bf16[2048,1408]{1,0:T(8,128)(2,1)}) %all-gather.11.cloned.1.call-update) | async-done | bytes 5767184 | tf_op jit(solution)/shard_map/all_gather | solution.py:184
  262.0 92.6 %all-gather.9.cloned.1.call-done = bf16[2048,1408]{1,0:T(8,128)(2,1)} async-done(((bf16[256,1408]{1,0:T(8,128)(2,1)}), bf16[2048,1408]{1,0:T(8,128)(2,1)}) %all-gather.9.cloned.1.call-update) | async-done | bytes 5767184 | tf_op jit(solution)/shard_map/all_gather | solution.py:183
  354.6 16.8 %convolution_convert_fusion.4 = bf16[768,2048]{1,0:T(8,128)(2,1)} fusion(bf16[2048,1408]{1,0:T(8,128)(2,1)} %all-gather.11.cloned.1.call-done, f32[768,1408]{1,0:T(8,128)} %fusion.42, bf16[2048,1408]{1,0:T(8,128)(2,1)} %all-gather.9.cloned.1.call-done, bf16[1536,2048]{1,0:T(8,128)(2,1)} %constant_dynamic-update-slice_fusion, s32[]{:T(128)S(6)} %select_n.49), kind=kOutput, calls=%fused_computation.50 | convolution fusion | flops 8866430976 | bytes 22151172 | tf_op jit(solution)/shard_map/dot_general | solution.py:196
  371.4 36.2 %reduce-scatter.2.cloned.1.call-done = bf16[192,2048]{1,0:T(8,128)(2,1)} async-done(((bf16[768,2048]{1,0:T(8,128)(2,1)}), bf16[192,2048]{1,0:T(8,128)(2,1)}) %reduce-scatter.2.cloned.1.call-update) | async-done | bytes 786448 | tf_op jit(solution)/shard_map/reduce_scatter | solution.py:195
  407.6 2.2 add_convert_fusion
  (46 shorter events, 0.4 us)
Async XLA Ops:
  6.5 7.2 %copy-start.4 = (bf16[768,192]{0,1:T(8,128)(2,1)S(1)}, bf16[768,192]{0,1:T(8,128)(2,1)}, u32[]{:S(2)}) copy-start(bf16[768,192]{0,1:T(8,128)(2,1)} %param.20) | copy-start | bytes 884740
  6.5 7.3 %copy-start.5 = (bf16[768,32]{0,1:T(8,128)(2,1)S(1)}, bf16[768,32]{0,1:T(8,128)(2,1)}, u32[]{:S(2)}) copy-start(bf16[768,32]{0,1:T(8,128)(2,1)} %param.23) | copy-start | bytes 147460
  6.5 69.2 %copy-start.2 = (bf16[256,128]{1,0:T(8,128)(2,1)S(1)}, bf16[256,128]{1,0:T(8,128)(2,1)}, u32[]{:S(2)}) copy-start(bf16[256,128]{1,0:T(8,128)(2,1)} %param.25) | copy-start | bytes 196612
  6.5 69.2 %copy-start.3 = (bf16[256,128]{1,0:T(8,128)(2,1)S(1)}, bf16[256,128]{1,0:T(8,128)(2,1)}, u32[]{:S(2)}) copy-start(bf16[256,128]{1,0:T(8,128)(2,1)} %param.26) | copy-start | bytes 196612
  6.5 69.2 %copy-start = (bf16[256,256]{1,0:T(8,128)(2,1)S(1)}, bf16[256,256]{1,0:T(8,128)(2,1)}, u32[]{:S(2)}) copy-start(bf16[256,256]{1,0:T(8,128)(2,1)} %param.27) | copy-start | bytes 393220
  6.5 69.2 %copy-start.1 = (bf16[256,256]{1,0:T(8,128)(2,1)S(1)}, bf16[256,256]{1,0:T(8,128)(2,1)}, u32[]{:S(2)}) copy-start(bf16[256,256]{1,0:T(8,128)(2,1)} %param.28) | copy-start | bytes 393220
  6.6 69.0 %all-gather.5.cloned.1.call-start = ((), (), s32[]{:S(2)}) async-start(), calls=%async_computation.3 | async-start | bytes 3538944 | tf_op jit(solution)/shard_map/all_gather | solution.py:154
  10.4 158.8 %all-gather.7.cloned.1.call-start = ((), (), s32[]{:S(2)}) async-start(), calls=%async_computation.4 | async-start | bytes 6488064 | tf_op jit(solution)/shard_map/all_gather | solution.py:182
  11.2 250.8 %all-gather.11.cloned.1.call-start = ((), (), s32[]{:S(2)}) async-start(), calls=%async_computation.6 | async-start | bytes 6488064 | tf_op jit(solution)/shard_map/all_gather | solution.py:184
  11.9 342.6 %all-gather.9.cloned.1.call-start = ((), (), s32[]{:S(2)}) async-start(), calls=%async_computation.5 | async-start | bytes 6488064 | tf_op jit(solution)/shard_map/all_gather | solution.py:183
  75.8 20.5 %copy-start.6 = (bf16[2048]{0:T(1024)(128)(2,1)S(1)}, bf16[2048]{0:T(1024)(128)(2,1)}, u32[]{:S(2)}) copy-start(bf16[2048]{0:T(1024)(128)(2,1)} %param.30) | copy-start | bytes 12292
  92.8 10.8 %all-to-all-start.1 = ((bf16[4,192,256]{2,1,0:T(8,128)(2,1)}), bf16[4,192,256]{2,1,0:T(8,128)(2,1)S(1)}, u32[]{:S(2)}, u32[]{:S(2)}) async-start(bf16[4,192,256]{2,1,0:T(8,128)(2,1)} %convert_element_type.152), calls=%async_computation.1 | async-start | bytes 786432 | tf_op jit(solution)/shard_map/all_to_all | solution.py:175
  103.6 8.8 %all-to-all-start = ((bf16[4,192,128]{2,1,0:T(8,128)(2,1)}), bf16[4,192,128]{2,1,0:T(8,128)(2,1)S(1)}, u32[]{:S(2)}, u32[]{:S(2)}) async-start(bf16[4,192,128]{2,1,0:T(8,128)(2,1)} %copy.34), calls=%async_computation | async-start | bytes 393216 | tf_op jit(solution)/shard_map/all_to_all | solution.py:174
  107.2 300.4 %reduce-scatter.2.cloned.1.call-start = ((), (), s32[]{:S(2)}) async-start(), calls=%async_computation.7 | async-start | bytes 3932160 | tf_op jit(solution)/shard_map/reduce_scatter | solution.py:195
  115.3 11.5 %collective-permute-start = (bf16[192,2048]{1,0:T(8,128)(2,1)S(1)}, bf16[192,2048]{1,0:T(8,128)(2,1)S(1)}, u32[]{:S(2)}, u32[]{:S(2)}) collective-permute-start(bf16[192,2048]{1,0:T(8,128)(2,1)S(1)} %multiply_convert_fusion.1), channel_id=1, source_target_pairs={{0,1},{1,2},{2,3},{3,0},{4,5},{5,6},{6,7},{7,4},{8,9},{9,10},{10,1... | collective-permute-start | bytes 2359304 | tf_op jit(solution)/shard_map/ppermute | solution.py:188
  126.7 11.4 %collective-permute-start.1 = (bf16[192,2048]{1,0:T(8,128)(2,1)S(1)}, bf16[192,2048]{1,0:T(8,128)(2,1)S(1)}, u32[]{:S(2)}, u32[]{:S(2)}) collective-permute-start(bf16[192,2048]{1,0:T(8,128)(2,1)S(1)} %collective-permute-done), channel_id=1, source_target_pairs={{0,1},{1,2},{2,3},{3,0},{4,5},{5,6},{6,7},{7,4},{8,9},{9,10},{10,1... | collective-permute-start | bytes 2359304 | tf_op jit(solution)/shard_map/ppermute | solution.py:188
  138.1 11.5 %collective-permute-start.2 = (bf16[192,2048]{1,0:T(8,128)(2,1)S(1)}, bf16[192,2048]{1,0:T(8,128)(2,1)}, u32[]{:S(2)}, u32[]{:S(2)}) collective-permute-start(bf16[192,2048]{1,0:T(8,128)(2,1)S(1)} %collective-permute-done.1), channel_id=1, source_target_pairs={{0,1},{1,2},{2,3},{3,0},{4,5},{5,6},{6,7},{7,4},{8,9},{9,10},{10,1... | collective-permute-start | bytes 2359304 | tf_op jit(solution)/shard_map/ppermute | solution.py:188
Sparse Core Ops, SparseCore 0:
  10.6 64.9 all-gather.4
  77.8 91.4 all-gather.6
  171.5 90.4 all-gather.10
  264.0 90.4 all-gather.8
  371.5 36.0 reduce-scatter.1
